TPU v7x, 256 devices: a 4x2x16 block of a 4x16x16 slice. The times are simulated.
256 devices in a mesh: grp: 2 (over y), sp: 16 (over z), tp: 8 (over x, core).
Axes of the slice: x: 4, y: 2, z: 16, core: 2. Of those that a mesh axis runs over, the one named last changes fastest.
The devices are a block of a 4x16x16 slice.
Arguments:
- tokens: bfloat16 [32, 4096, 4096], P(('grp', 'tp'), 'sp'), parts along dimension 0, may hold values from -8 to 8, as said below
- offsets: int32 [32], P(('grp', 'tp')), parts along dimension 0, may hold values from 0 to 4095
- in_gain: float32 [4096], replicated, may hold values from 0.1 to 1.9
- w_latent: bfloat16 [4096, 1024], P('sp'), may hold values from -0.09375 to 0.09375
- w_rope_key: bfloat16 [4096, 32], replicated, may hold values from -0.09375 to 0.09375
- kv_gain: float32 [1024], replicated, may hold values from 0.1 to 1.9
- w_up_key: bfloat16 [1024, 2048], P(None, 'tp'), may hold values from -0.1875 to 0.1875
- w_up_value: bfloat16 [1024, 2048], P(None, 'tp'), may hold values from -0.1875 to 0.1875
- q_nope: bfloat16 [32, 2048], P(('grp', 'sp'), 'tp'), parts along dimension 0, may hold values from -300 to 300, as said below
- q_rope: bfloat16 [32, 1024], P(('grp', 'sp'), 'tp'), parts along dimension 0, may hold values from -16 to 16
Outputs:
- keys: bfloat16 [32, 4096, 2048], P(('grp', 'sp'), None, 'tp'), parts along dimension 0
- values: bfloat16 [32, 4096, 2048], P(('grp', 'sp'), None, 'tp'), parts along dimension 0
- rope_keys: bfloat16 [32, 32, 4096], P(('grp', 'sp')), parts along dimension 0
- read: bfloat16 [32, 2048], P(('grp', 'sp'), 'tp'), parts along dimension 0
There are 2 independent parts, one for each index of `grp`. A program takes and returns all parts, laid end to end along the dimension named above; an argument that names none is the same for every part. Nothing has to cross between parts.
Inputs may be any that keep to these rules, and one draw needn't show every extreme that they name: `tokens`: entries of the layer's input. `q_nope`: entries of the first decoding token's queries.
All inputs are finite; a program needn't handle non-finite values.
Results may differ from a plain program's by a relative error of at most 0.02.
Values may be sent and summed in bfloat16 or wider, within the bound.
A program may use at most 128 MiB of HBM per device.

v0:
```python
import functools

import jax
import jax.numpy as jnp
from jax import lax
from jax.experimental import pallas as pl
from jax.experimental.pallas import tpu as pltpu
from jax.sharding import PartitionSpec as P

HEAD = 64
ROPE = 32
EPS = 1e-06
MESH = pl.DeviceIdType.MESH
WX = 5
FULL = 96

LAGS = (1, 3, 4)
HALVES = 2
PARTS = (2, 3)


def exchange(
    n_sp, n_tp, tok_hbm, off_ref, gain_hbm, wl_hbm, wrope_hbm, kvg_hbm, wk_hbm, wv_hbm,
    keys_ref, values_ref, rope_ref,
    norm, wfull, wup, lat, acc, latall, ropeown, stage, gain_ref, wrope_ref, kvg_ref,
    local_sem, wz_sem, wx_sem, wp_sem, wsend, a_sem, dir_sem, lx_sem, lp_sem, lsend, rsem, rsend,
):
    z = lax.axis_index("sp")
    t = lax.axis_index("tp")
    n_x = n_tp // 2
    x, c = t // 2, lax.rem(t, 2)
    rows = norm.shape[0] // 2
    width = norm.shape[1]
    rank = lat.shape[1]
    depth = width // n_sp
    quarter = rank // n_x
    piece = rows // n_x
    heads = keys_ref.shape[1]

    def wrap(v, n):
        return lax.rem(v + 2 * n, n)

    def dev(xx, cc, zz):
        return {"sp": zz, "tp": 2 * xx + cc}

    z_next, z_prev = wrap(z + 1, n_sp), wrap(z - 1, n_sp)
    right = dev(wrap(x + 1, n_x), c, z)
    left = dev(wrap(x - 1, n_x), c, z)
    up = dev(x, c, z_next)
    down = dev(x, c, z_prev)
    partner = dev(x, 1 - c, z)
    home = lax.rem(z, 2)
    src_x, src_c = z // 4, lax.rem(z // 2, 2)
    has_self = jnp.logical_and(src_c == c, c == home)

    loads = [
        pltpu.make_async_copy(wl_hbm, wfull.at[pl.ds(z * depth, depth)], local_sem.at[0]),
        pltpu.make_async_copy(tok_hbm, norm, local_sem.at[1]),
        pltpu.make_async_copy(wk_hbm, wup.at[:, pl.ds(0, heads)], local_sem.at[2]),
        pltpu.make_async_copy(wv_hbm, wup.at[:, pl.ds(heads, heads)], local_sem.at[3]),
        pltpu.make_async_copy(gain_hbm, gain_ref, local_sem.at[4]),
        pltpu.make_async_copy(wrope_hbm, wrope_ref, local_sem.at[5]),
        pltpu.make_async_copy(kvg_hbm, kvg_ref, local_sem.at[6]),
    ]
    for load in loads:
        load.start()

    barrier = pltpu.get_barrier_semaphore()

    def greet(device):
        pl.semaphore_signal(barrier, inc=1, device_id=device, device_id_type=MESH)

    column = lax.rem(z // 2, n_x)
    rope_self = jnp.logical_and(jnp.logical_and(x == src_x, c == src_c), jnp.logical_and(x == column, c == home))
    around = (right, left, up, down, partner)
    for device in around:
        greet(device)
    pl.semaphore_wait(barrier, len(around))

    def send(src, dst, device, send_sem, recv_sem):
        pltpu.make_async_remote_copy(
            src_ref=src, dst_ref=dst, send_sem=send_sem, recv_sem=recv_sem,
            device_id=device, device_id_type=MESH,
        ).start()

    def arrived(dst, recv_sem):
        pltpu.make_async_copy(dst, dst, recv_sem).wait()

    sign = 1 - 2 * c
    onward = dev(x, c, wrap(z + sign, n_sp))
    ahead, behind = dev(wrap(x + sign, n_x), c, z), dev(wrap(x - sign, n_x), c, z)
    q_part, f_part = (depth - FULL) // PARTS[0], FULL // PARTS[1]
    parts = [("q", i) for i in range(PARTS[0])] + [("f", i) for i in range(PARTS[1])]

    def w_part(s, xx):
        return wfull.at[
            pl.ds(pl.multiple_of(s * depth + FULL, 32), depth - FULL),
            pl.ds(pl.multiple_of(xx * quarter, quarter), quarter),
        ]

    def w_message(s, kind, i):
        if kind == "f":
            return wfull.at[pl.ds(pl.multiple_of(s * depth + i * f_part, f_part), f_part)]
        return wfull.at[
            pl.ds(pl.multiple_of(s * depth + FULL + i * q_part, 16), q_part),
            pl.ds(pl.multiple_of(x * quarter, quarter), quarter),
        ]

    def w_shard(s, first=0, size=depth):
        return wfull.at[pl.ds(pl.multiple_of(s * depth + first, 32), size)]

    steps = n_sp // 2
    owner = {"f": 0, "q": 1}

    def when_due(k, kind, action):
        if k < steps:
            action()
        elif k == steps:
            pl.when(c == owner[kind])(action)

    def z_send(part, k):
        ref = w_message(wrap(z - sign * k, n_sp), *part)
        row = parts.index(part)
        send(ref, ref, onward, wsend.at[row], wz_sem.at[row, k])

    def z_arrive(part, k):
        kind, i = part
        s = wrap(z - sign * k, n_sp)
        arrived(w_message(s, *part), wz_sem.at[parts.index(part), k - 1])
        when_due(k + 1, kind, functools.partial(z_send, part, k))
        if kind == "q" and i == PARTS[0] - 1:
            ref = w_part(s, x)
            send(ref, ref, ahead, wsend.at[WX], wx_sem.at[0, k - 1])
            send(ref, ref, behind, wsend.at[WX + 1], wx_sem.at[1, k - 1])

    def x_arrive(k):
        s = wrap(z - sign * k, n_sp)
        from_behind = w_part(s, wrap(x - sign, n_x))
        arrived(from_behind, wx_sem.at[0, k - 1])
        send(from_behind, from_behind, ahead, wsend.at[WX + 2], wx_sem.at[2, k - 1])
        arrived(w_part(s, wrap(x + sign, n_x)), wx_sem.at[1, k - 1])

    def hand_over(ref, k):
        send(ref, ref, partner, wsend.at[WX + 3], wp_sem.at[k - 1])

    def far_arrive(k):
        s = wrap(z - sign * k, n_sp)
        arrived(w_part(s, wrap(x + 2, n_x)), wx_sem.at[2, k - 1])
        if k < steps:
            hand_over(w_shard(s), k)
        else:
            hand_over(w_shard(s, FULL, depth - FULL), k)

    loads[0].wait()
    if True:
        for part in parts:
            z_send(part, 0)

    loads[1].wait()
    loads[4].wait()
    loads[5].wait()
    loads[6].wait()

    def normalise(part, parts):
        @pl.loop(part * 2 * rows // 32 // parts, (part + 1) * 2 * rows // 32 // parts)
        def _(n):
            r = pl.ds(pl.multiple_of(n * 32, 32), 32)
            wide = norm[r, :].astype(jnp.float32)
            scale = lax.rsqrt(jnp.sum(wide * wide, axis=-1, keepdims=True) * (1.0 / width) + EPS)
            norm[r, :] = (wide * scale * gain_ref[...]).astype(jnp.bfloat16)

    def partial(s, first=False):
        @pl.loop(0, n_x)
        def _(n):
            cols = pl.ds(pl.multiple_of(n * quarter, quarter), quarter)
            term = jnp.dot(
                norm[:, pl.ds(pl.multiple_of(s * depth, depth), depth)],
                wfull[pl.ds(pl.multiple_of(s * depth, depth), depth), cols],
                preferred_element_type=jnp.float32,
            )
            acc[:, cols] = term if first else acc[:, cols] + term

    def finish(k):
        s = wrap(z + sign * k, n_sp)
        if k < steps:
            arrived(w_shard(s), wp_sem.at[k - 1])
            partial(wrap(z - sign * k, n_sp))
        else:
            pl.when(c == 0)(lambda: arrived(w_shard(s, FULL, depth - FULL), wp_sem.at[k - 1]))
            pl.when(c == 1)(lambda: arrived(w_shard(s, 0, FULL), wp_sem.at[k - 1]))
        partial(s)

    def rotary():
        raw = lax.dot_general(
            wrope_ref[...], norm[...], (((1,), (1,)), ((), ())), preferred_element_type=jnp.float32
        )
        index = lax.broadcasted_iota(jnp.int32, (ROPE // 2, rows), 0).astype(jnp.float32) * 2.0
        inverse = jnp.exp(index * (-jnp.log(jnp.float32(10000.0)) / ROPE))
        place = lax.broadcasted_iota(jnp.int32, (ROPE // 2, rows), 1)
        for j in range(2):
            angle = (off_ref[j] + z * rows + place).astype(jnp.float32) * inverse
            cosine, sine = jnp.cos(angle), jnp.sin(angle)
            first = raw[: ROPE // 2, j * rows:(j + 1) * rows]
            second = raw[ROPE // 2:, j * rows:(j + 1) * rows]
            ropeown[j] = jnp.concatenate(
                [first * cosine - second * sine, second * cosine + first * sine], axis=0
            ).astype(jnp.bfloat16)

    def follow(k):
        for lag, action in zip(LAGS, (x_arrive, far_arrive, finish)):
            if 1 <= k - lag <= steps:
                step = functools.partial(action, k - lag)
                if action is finish:
                    step()
                else:
                    when_due(k - lag, "q", step)
        if k == 3:
            partial(z, True)
        if k == 4:
            rotary()

    normalise(0, 4)
    for k in range(1, steps + 1):
        for part in parts:
            when_due(k, part[0], functools.partial(z_arrive, part, k))
        if k == steps:
            pl.when(c == 0)(lambda: hand_over(w_shard(wrap(z + steps, n_sp), 0, FULL), steps))
        if k < 4:
            normalise(k, 4)
        follow(k)
    for k in range(steps + 1, steps + LAGS[2] + 1):
        follow(k)

    for j in range(2):
        own = jnp.logical_and(rope_self, 2 * t + j == z)
        dst = rope_ref.at[:, pl.ds(pl.multiple_of(z * rows, rows), rows)]

        @pl.when(own)
        def _():
            pltpu.make_async_copy(ropeown.at[j], dst, rsem.at[z]).start()

        @pl.when(jnp.logical_not(own))
        def _():
            send(ropeown.at[j], dst, dev(column, home, 2 * t + j), rsend.at[0, j], rsem.at[z])

    small = piece // HALVES

    def own_piece(j, q, h):
        return lat.at[pl.ds(pl.multiple_of(j * rows + (h * n_x + q) * small, small), small)]

    def staged(xx, j, h):
        return stage.at[xx, j, pl.ds(h * small, small)]

    def place_of(s, q, h):
        return latall.at[pl.ds(pl.multiple_of(s * rows + (h * n_x + q) * small, small), small)]

    @pl.loop(0, 2 * rows // 64)
    def _(n):
        r = pl.ds(pl.multiple_of(n * 64, 64), 64)
        wide = acc[r, :]
        scale = lax.rsqrt(jnp.sum(wide * wide, axis=-1, keepdims=True) * (1.0 / rank) + EPS)
        lat[r, :] = (wide * scale * kvg_ref[...]).astype(jnp.bfloat16)

    for h in range(HALVES):
        for j in range(2):
            for d in (2, 1, -1):
                q = wrap(x + d, n_x)
                send(own_piece(j, q, h), staged(x, j, h), dev(q, c, z), lsend.at[0, j], a_sem.at[x, j, h])
    for h in range(HALVES):
        for j in range(2):
            stage[x, j, pl.ds(h * small, small)] = lat[
                pl.ds(pl.multiple_of(j * rows + (h * n_x + x) * small, small), small), :
            ]

    origin = lax.rem(z - 2 * c + n_sp, n_sp) // 4
    for h in range(HALVES):
        for d in (0, 1, -1, 2):
            xx = wrap(origin + d, n_x)
            for j in range(2):
                goal = 4 * xx + 2 * c + j
                own = jnp.logical_and(has_self, goal == z)

                @pl.when(xx != x)
                def _():
                    arrived(staged(xx, j, h), a_sem.at[xx, j, h])

                src, dst, sem = staged(xx, j, h), place_of(z, x, h), dir_sem.at[z // 2, h]

                @pl.when(own)
                def _():
                    pltpu.make_async_copy(src, dst, sem).start()

                @pl.when(jnp.logical_not(own))
                def _():
                    send(src, dst, dev(x, home, goal), lsend.at[3, 0], sem)

    near = [0] + [v for k in range(2, steps, 2) for v in (k, -k)] + [steps]
    odd = [v for k in range(1, steps, 2) for v in (k, -k)]
    same = home == c
    sources = [wrap(z + jnp.where(same, a, b), n_sp) for a, b in zip(near, odd)]
    other = [wrap(z + jnp.where(same, b, a), n_sp) for a, b in zip(near, odd)]
    n_src = len(sources)

    def direct(n, h):
        s = sources[n]
        ref = place_of(s, x, h)
        arrived(ref, dir_sem.at[s // 2, h])
        send(ref, ref, right, lsend.at[1, 0], lx_sem.at[0, n, h])
        send(ref, ref, left, lsend.at[1, 1], lx_sem.at[1, n, h])

    def beside(n, h):
        s = sources[n]
        from_left, from_right = place_of(s, wrap(x - 1, n_x), h), place_of(s, wrap(x + 1, n_x), h)
        arrived(from_left, lx_sem.at[0, n, h])
        if (n + h) % 2 == 0:
            send(from_left, from_left, right, lsend.at[2, 0], lx_sem.at[2, n, h])
        arrived(from_right, lx_sem.at[1, n, h])
        if (n + h) % 2 == 1:
            send(from_right, from_right, left, lsend.at[2, 0], lx_sem.at[2, n, h])

    def block(s, h):
        return latall.at[pl.ds(pl.multiple_of(s * rows + h * n_x * small, small), n_x * small)]

    def far(n, h):
        s = sources[n]
        arrived(place_of(s, wrap(x + 2, n_x), h), lx_sem.at[2, n, h])
        send(block(s, h), block(s, h), partner, lsend.at[2, 1], lp_sem.at[s, h])

    def up_project(s, h):
        r = pl.ds(pl.multiple_of(s * rows + h * n_x * small, small), n_x * small)
        both = jnp.dot(latall[r, :], wup[...], preferred_element_type=jnp.float32).astype(jnp.bfloat16)
        keys_ref[r, :] = both[:, :heads]
        values_ref[r, :] = both[:, heads:]

    def rope_block(s):
        return rope_ref.at[:, pl.ds(pl.multiple_of(s * rows, rows), rows)]

    peers = [(dx, dc) for dx in range(n_x) for dc in range(2) if dx or dc]
    def rope_onward():
        for g in range(n_sp // 2 // n_x):
            s = 2 * (x + n_x * g) + c
            arrived(rope_block(s), rsem.at[s])
            for n, (dx, dc) in enumerate(peers):
                send(
                    rope_block(s), rope_block(s), dev(wrap(x + dx, n_x), lax.rem(c + dc, 2), z),
                    rsend.at[1 + g, n], rsem.at[s],
                )

    loads[2].wait()
    loads[3].wait()
    order = [(n, h) for h in range(HALVES) for n in range(n_src)]

    def other_half(n, h):
        s = other[n]
        arrived(block(s, h), lp_sem.at[s, h])
        up_project(s, h)

    def far_half(n, h):
        far(n, h)
        up_project(sources[n], h)

    actions = ((0, direct), (2, beside), (5, far_half), (6, other_half))
    for i in range(len(order) + 6):
        for lag, action in actions:
            if 0 <= i - lag < len(order):
                action(*order[i - lag])
        if i == 6:
            rope_onward()

    for s in range(n_sp):
        mine = jnp.logical_and(lax.rem(s // 2, n_x) == x, s % 2 == c)

        @pl.when(jnp.logical_not(mine))
        def _():
            arrived(rope_block(s), rsem.at[s])

    for j in range(2):
        own = jnp.logical_and(rope_self, 2 * t + j == z)

        @pl.when(jnp.logical_not(own))
        def _():
            arrived(ropeown.at[j], rsend.at[0, j])

    for g in range(n_sp // 2 // n_x):
        for n in range(len(peers)):
            arrived(ropeown.at[0], rsend.at[1 + g, n])
    for core in range(2):
        @pl.when(c == core)
        def _():
            trips = {kind: steps - (owner[kind] != core) for kind in owner}
            for row, (kind, _) in enumerate(parts):
                if kind == "f":
                    arrived(wfull.at[pl.ds(0, trips[kind] * f_part)], wsend.at[row])
                else:
                    arrived(wfull.at[pl.ds(0, trips[kind] * q_part), pl.ds(0, quarter)], wsend.at[row])
            for row in range(WX, WX + 3):
                arrived(wfull.at[pl.ds(0, trips["q"] * (depth - FULL)), pl.ds(0, quarter)], wsend.at[row])
            last = FULL if core == 0 else depth - FULL
            arrived(wfull.at[pl.ds(0, (steps - 1) * depth + last)], wsend.at[WX + 3])

    if True:
        for j in range(2):
            arrived(lat.at[pl.ds(0, rows - piece)], lsend.at[0, j])
        pl.when(has_self)(lambda: arrived(lat.at[pl.ds(0, 2 * rows - piece)], lsend.at[3, 0]))
        pl.when(jnp.logical_not(has_self))(lambda: arrived(lat, lsend.at[3, 0]))
        for a, b in ((1, 0), (1, 1), (2, 0)):
            arrived(latall.at[pl.ds(0, n_src * piece)], lsend.at[a, b])
        arrived(latall.at[pl.ds(0, n_src * rows)], lsend.at[2, 1])


def in_hbm(value):
    return pltpu.with_memory_space_constraint(value, pltpu.HBM)


def attend(
    keys_ref, values_ref, rope_ref, qn_ref, qr_ref, keys_out, values_out, rope_out, read_ref, sem
):
    outs = [
        pltpu.make_async_copy(keys_ref, keys_out, sem.at[0]),
        pltpu.make_async_copy(values_ref, values_out, sem.at[1]),
        pltpu.make_async_copy(rope_ref, rope_out, sem.at[2]),
    ]
    for out in outs:
        out.start()
    heads = keys_ref.shape[1] // HEAD
    rot = qr_ref.shape[1] // heads
    pad = 8

    def by_head(ref, size):
        wide = jnp.broadcast_to(ref[...].astype(jnp.float32), (pad, ref.shape[1]))
        row = lax.broadcasted_iota(jnp.int32, wide.shape, 0)
        col = lax.broadcasted_iota(jnp.int32, wide.shape, 1)
        return jnp.where(col // size == row, wide, 0.0)

    nope = by_head(qn_ref, HEAD).astype(jnp.bfloat16)
    scores = lax.dot_general(
        nope, keys_ref[...], (((1,), (1,)), ((), ())), preferred_element_type=jnp.float32
    )
    spread = by_head(qr_ref, rot)
    rotary = spread[:, :rot]
    for h in range(1, heads):
        rotary = rotary + spread[:, h * rot:(h + 1) * rot]
    scores = scores + jnp.dot(
        rotary.astype(jnp.bfloat16), rope_ref[...], preferred_element_type=jnp.float32
    )
    scores = scores / jnp.sqrt(jnp.float32(HEAD + ROPE))
    expo = jnp.exp(scores - jnp.max(scores, axis=-1, keepdims=True))
    weights = (expo / jnp.sum(expo, axis=-1, keepdims=True)).astype(jnp.bfloat16)
    read = jnp.dot(weights, values_ref[...], preferred_element_type=jnp.float32)
    row = lax.broadcasted_iota(jnp.int32, read.shape, 0)
    col = lax.broadcasted_iota(jnp.int32, read.shape, 1)
    read_ref[...] = jnp.sum(
        jnp.where(col // HEAD == row, read, 0.0), axis=0, keepdims=True
    ).astype(jnp.bfloat16)
    for out in outs:
        out.wait()


def local(
    n_sp, n_tp,
    tokens, offsets, in_gain, w_latent, w_rope_key, kv_gain, w_up_key, w_up_value, q_nope, q_rope
):
    prompts, rows, width = tokens.shape
    depth, rank = w_latent.shape
    heads = w_up_key.shape[1]
    length = n_sp * rows
    steps = n_sp // 2
    any_space = pl.BlockSpec(memory_space=pl.ANY)
    hbm = pl.BlockSpec(memory_space=pltpu.HBM)
    vmem = pl.BlockSpec(memory_space=pltpu.VMEM)
    smem = pl.BlockSpec(memory_space=pltpu.SMEM)
    dma = pltpu.SemaphoreType.DMA
    keys, values, rope = pl.pallas_call(
        functools.partial(exchange, n_sp, n_tp),
        out_shape=(
            jax.ShapeDtypeStruct((length, heads), jnp.bfloat16),
            jax.ShapeDtypeStruct((length, heads), jnp.bfloat16),
            jax.ShapeDtypeStruct((ROPE, length), jnp.bfloat16),
        ),
        in_specs=[hbm, smem, hbm, hbm, hbm, hbm, hbm, hbm],
        out_specs=(vmem, vmem, vmem),
        scratch_shapes=[
            pltpu.VMEM((prompts * rows, width), jnp.bfloat16),
            pltpu.VMEM((width, rank), jnp.bfloat16),
            pltpu.VMEM((rank, 2 * heads), jnp.bfloat16),
            pltpu.VMEM((prompts * rows, rank), jnp.bfloat16),
            pltpu.VMEM((prompts * rows, rank), jnp.float32),
            pltpu.VMEM((length, rank), jnp.bfloat16),
            pltpu.VMEM((prompts, ROPE, rows), jnp.bfloat16),
            pltpu.VMEM((n_tp // 2, prompts, rows * 2 // n_tp, rank), jnp.bfloat16),
            pltpu.VMEM((1, width), jnp.float32),
            pltpu.VMEM((ROPE, width), jnp.bfloat16),
            pltpu.VMEM((1, rank), jnp.float32),
            dma((7,)),
            dma((WX, steps)),
            dma((3, steps)),
            dma((steps,)),
            dma((WX + 4,)),
            dma((n_tp // 2, prompts, HALVES)),
            dma((steps, HALVES)),
            dma((3, steps, HALVES)),
            dma((n_sp, HALVES)),
            dma((4, 2)),
            dma((n_sp,)),
            dma((1 + n_sp // n_tp, n_tp - 1)),
        ],
        compiler_params=pltpu.CompilerParams(
            collective_id=0, has_side_effects=True, vmem_limit_bytes=40 * 1024 * 1024
        ),
        name="exchange",
    )(
        *map(
            in_hbm,
            (tokens.reshape(prompts * rows, width),),
        ),
        offsets,
        *map(
            in_hbm,
            (
                in_gain.reshape(1, width), w_latent, w_rope_key.T, kv_gain.reshape(1, rank),
                w_up_key, w_up_value,
            ),
        ),
    )
    return pl.pallas_call(
        attend,
        out_shape=(
            jax.ShapeDtypeStruct((length, heads), jnp.bfloat16),
            jax.ShapeDtypeStruct((length, heads), jnp.bfloat16),
            jax.ShapeDtypeStruct((ROPE, length), jnp.bfloat16),
            jax.ShapeDtypeStruct((1, heads), jnp.bfloat16),
        ),
        in_specs=[vmem] * 5,
        out_specs=(any_space, any_space, any_space, vmem),
        scratch_shapes=[dma((3,))],
        compiler_params=pltpu.CompilerParams(vmem_limit_bytes=24 * 1024 * 1024),
        name="attend",
    )(keys, values, rope, q_nope, q_rope)


def solution(mesh):
    n_sp, n_tp = mesh.shape["sp"], mesh.shape["tp"]

    def body(*args):
        keys, values, rope, read = local(n_sp, n_tp, *args)
        return keys[None], values[None], rope[None], read

    in_specs = (
        P(("grp", "tp"), "sp", None),
        P(("grp", "tp")),
        P(),
        P("sp", None),
        P(),
        P(),
        P(None, "tp"),
        P(None, "tp"),
        P(("grp", "sp"), "tp"),
        P(("grp", "sp"), "tp"),
    )
    out_specs = (
        P(("grp", "sp"), None, "tp"),
        P(("grp", "sp"), None, "tp"),
        P(("grp", "sp"), None, None),
        P(("grp", "sp"), "tp"),
    )
    return jax.shard_map(body, mesh=mesh, in_specs=in_specs, out_specs=out_specs, check_vma=False)
```

profile of v0, /device:TPU:163, one launch (start us, length us, event | category | flops | bytes accessed | tf_op | source)
XLA Modules:
  0.0 138.8 jit_solution(9925669621595943480)
XLA Ops:
  0.6 0.0 copy-start.1
  0.6 0.6 copy-done.1
  1.3 0.0 copy-start
  1.3 0.0 copy-start.2
  1.3 134.4 %exchange.1 = (bf16[4096,256]{1,0:T(8,128)(2,1)S(1)}, bf16[4096,256]{1,0:T(8,128)(2,1)S(1)}, bf16[32,4096]{1,0:T(8,128)(2,1)S(1)}) custom-call(bf16[512,4096]{1,0:T(8,128)(2,1)} %bitcast.7, s32[2]{0:T(128)S(1)} %copy-done.1, f32[1,4096]{1,0:T(1,128)} %bitcast.9, bf16[256,1024]{1,0:T(8,128)(2,1)} %wl_hbm.1, bf16[32,4096]{1,0:T(8,128)(2,1)} %bitcast.8, ...), custom_call_target="tpu_custom_call" | custom-call | tf_op jit(solution)/shard_map/exchange/pallas_call | solution.py:473
  135.7 0.0 copy-done
  135.7 0.0 copy-done.2
  135.7 2.9 %attend.1 = (bf16[4096,256]{1,0:T(8,128)(2,1)}, bf16[4096,256]{1,0:T(8,128)(2,1)}, bf16[32,4096]{1,0:T(8,128)(2,1)}, bf16[1,256]{1,0:T(2,128)(2,1)}) custom-call(bf16[4096,256]{1,0:T(8,128)(2,1)S(1)} %get-tuple-element.11.keys_ref, bf16[4096,256]{1,0:T(8,128)(2,1)S(1)} %get-tuple-element.12.values_ref, bf16[32,4096]{1,0:T(8,128)(2,1)S(1)} %get-tuple-element.13.rope_ref, ...), custom_call_target="tpu_custom_call" | custom-call | tf_op jit(solution)/shard_map/attend/pallas_call | solution.py:525
Async XLA Ops:
  0.6 0.7 copy-start.1
  1.3 134.4 %copy-start = (bf16[1,256]{1,0:T(2,128)(2,1)S(1)}, bf16[1,256]{1,0:T(2,128)(2,1)}, u32[]{:S(2)}) copy-start(bf16[1,256]{1,0:T(2,128)(2,1)} %qn_ref.1) | copy-start | bytes 1540
  1.3 134.4 %copy-start.2 = (bf16[1,128]{1,0:T(2,128)(2,1)S(1)}, bf16[1,128]{1,0:T(2,128)(2,1)}, u32[]{:S(2)}) copy-start(bf16[1,128]{1,0:T(2,128)(2,1)} %qr_ref.1) | copy-start | bytes 772
where the time goes:
time: 139 us
  Pallas kernels  137 us (99%)
    pallas_call x1, Pallas kernels, local(): pl.pallas_call(functools.partial(exchange, n_sp, n_tp), out_shape=(jax.Sh...  134 us
    pallas_call x1, Pallas kernels, local(): pl.pallas_call(attend, out_shape=(jax.ShapeDtypeStruct((length, heads), j...  2.92 us

commit v1 on v0

--- a/solution.py
+++ b/solution.py
@@ -359,12 +359,12 @@
         far(n, h)
         up_project(sources[n], h)
 
-    actions = ((0, direct), (2, beside), (5, far_half), (6, other_half))
-    for i in range(len(order) + 6):
+    actions = ((0, direct), (3, beside), (6, far_half), (8, other_half))
+    for i in range(len(order) + 8):
         for lag, action in actions:
             if 0 <= i - lag < len(order):
                 action(*order[i - lag])
-        if i == 6:
+        if i == 9:
             rope_onward()
 
     for s in range(n_sp):

time: 139 us -> 139 us (level)
  no operation moved by 1% of the time
where the time goes in v1:
time: 139 us
  Pallas kernels  138 us (99%)
    pallas_call x1, Pallas kernels, local(): pl.pallas_call(functools.partial(exchange, n_sp, n_tp), out_shape=(jax.Sh...  135 us
    pallas_call x1, Pallas kernels, local(): pl.pallas_call(attend, out_shape=(jax.ShapeDtypeStruct((length, heads), j...  2.92 us

profile of v1, /device:TPU:163, one launch (start us, length us, event | category | flops | bytes accessed | tf_op | source)
XLA Modules:
  0.0 139.3 jit_solution(3377596212919570766)
XLA Ops:
  0.6 0.0 copy-start.1
  0.6 0.6 copy-done.1
  1.3 0.0 copy-start
  1.3 0.0 copy-start.2
  1.3 134.9 %exchange.1 = (bf16[4096,256]{1,0:T(8,128)(2,1)S(1)}, bf16[4096,256]{1,0:T(8,128)(2,1)S(1)}, bf16[32,4096]{1,0:T(8,128)(2,1)S(1)}) custom-call(bf16[512,4096]{1,0:T(8,128)(2,1)} %bitcast.7, s32[2]{0:T(128)S(1)} %copy-done.1, f32[1,4096]{1,0:T(1,128)} %bitcast.9, bf16[256,1024]{1,0:T(8,128)(2,1)} %wl_hbm.1, bf16[32,4096]{1,0:T(8,128)(2,1)} %bitcast.8, ...), custom_call_target="tpu_custom_call" | custom-call | tf_op jit(solution)/shard_map/exchange/pallas_call | solution.py:473
  136.2 0.0 copy-done
  136.3 0.0 copy-done.2
  136.3 2.9 %attend.1 = (bf16[4096,256]{1,0:T(8,128)(2,1)}, bf16[4096,256]{1,0:T(8,128)(2,1)}, bf16[32,4096]{1,0:T(8,128)(2,1)}, bf16[1,256]{1,0:T(2,128)(2,1)}) custom-call(bf16[4096,256]{1,0:T(8,128)(2,1)S(1)} %get-tuple-element.11.keys_ref, bf16[4096,256]{1,0:T(8,128)(2,1)S(1)} %get-tuple-element.12.values_ref, bf16[32,4096]{1,0:T(8,128)(2,1)S(1)} %get-tuple-element.13.rope_ref, ...), custom_call_target="tpu_custom_call" | custom-call | tf_op jit(solution)/shard_map/attend/pallas_call | solution.py:525
Async XLA Ops:
  0.6 0.7 copy-start.1
  1.3 135.0 %copy-start = (bf16[1,256]{1,0:T(2,128)(2,1)S(1)}, bf16[1,256]{1,0:T(2,128)(2,1)}, u32[]{:S(2)}) copy-start(bf16[1,256]{1,0:T(2,128)(2,1)} %qn_ref.1) | copy-start | bytes 1540
  1.3 135.0 %copy-start.2 = (bf16[1,128]{1,0:T(2,128)(2,1)S(1)}, bf16[1,128]{1,0:T(2,128)(2,1)}, u32[]{:S(2)}) copy-start(bf16[1,128]{1,0:T(2,128)(2,1)} %qr_ref.1) | copy-start | bytes 772
